TPU v7x, 512 devices: a 8x2x16 block of a 8x8x16 slice. The times are simulated.
512 devices in a mesh: grp: 2 (over y), sp: 16 (over z), tp: 16 (over x, core).
Axes of the slice: x: 8, y: 2, z: 16, core: 2. Of those that a mesh axis runs over, the one named last changes fastest.
The devices are a block of a 8x8x16 slice.
Arguments:
- target: bfloat16 [4096, 2048], P(('grp', 'sp', 'tp')), parts along dimension 0, may hold values from -5 to 5
- source: bfloat16 [32768, 2048], P(('grp', 'sp', 'tp')), parts along dimension 0, may hold values from -5 to 5
- source_gain: float32 [2048], replicated, may hold values from 0.1 to 1.9
- pre_first: float32 [2048], replicated, may hold values from 0.1 to 1.9
- query_first: bfloat16 [2048, 2048], P(None, 'tp')
- keyval_first: bfloat16 [2048, 1024], P(None, 'tp')
- out_first: bfloat16 [2048, 2048], P('tp'), may hold values from -0.125 to 0.125
- post_first: float32 [2048], replicated, may hold values from 0.1 to 1.9
- ffn_pre: float32 [2048], replicated, may hold values from 0.1 to 1.9
- w_gate: bfloat16 [2048, 2816], P(None, 'tp'), may hold values from -0.125 to 0.125
- w_value: bfloat16 [2048, 2816], P(None, 'tp'), may hold values from -0.125 to 0.125
- conv_gate: float32 [3, 2816], P(None, 'tp'), may hold values from -3.5 to 3.5
- conv_value: float32 [3, 2816], P(None, 'tp'), may hold values from -3.5 to 3.5
- w_down: bfloat16 [2816, 2048], P('tp'), may hold values from -0.109375 to 0.109375
- ffn_post: float32 [2048], replicated, may hold values from 0.1 to 1.9
- pre_second: float32 [2048], replicated, may hold values from 0.1 to 1.9
- query_second: bfloat16 [2048, 2048], P(None, 'tp')
- keyval_second: bfloat16 [2048, 1024], P(None, 'tp')
- out_second: bfloat16 [2048, 2048], P('tp'), may hold values from -0.125 to 0.125
- post_second: float32 [2048], replicated, may hold values from 0.1 to 1.9
Outputs:
- decoded: float32 [4096, 2048], P(('grp', 'sp', 'tp')), parts along dimension 0
There are 2 independent parts, one for each index of `grp`. A program takes and returns all parts, laid end to end along the dimension named above; an argument that names none is the same for every part. Nothing has to cross between parts.
All inputs are finite; a program needn't handle non-finite values.
Results may differ from a plain program's by a relative error of at most 0.04.
Values may be sent and summed in bfloat16 or wider, within the bound.
A program may use at most 128 MiB of HBM per device.

v0:
```python
import jax
import jax.numpy as jnp
from jax import lax
from jax.sharding import PartitionSpec as P

HEAD = 128
KVH = 4


def in_blocks(array, dim, size):
    before, after = (array.shape[:dim], array.shape[dim + 1 :])
    return jnp.moveaxis(array.reshape(*before, size, -1, *after), dim, 0)


def sent_and_summed(array, axis, dim):
    parts = in_blocks(array, dim, lax.axis_size(axis))
    arrived = lax.all_to_all(parts, axis, split_axis=0, concat_axis=0, tiled=True)
    return arrived.astype(jnp.float32).sum(axis=0)


def swapped(block, axis, distance):
    count = lax.axis_size(axis)
    route = []
    for low in range(count):
        high = low | 1 << distance
        if high != low and high < count:
            route += [(low, high), (high, low)]
    return lax.ppermute(block, axis, route)


def in_one_piece(arrays, axis, dim, along):
    both = jnp.concatenate(arrays, axis=along)
    result, at, done = (lax.all_gather(both, axis, axis=dim, tiled=True), 0, [])
    for a in arrays:
        done.append(lax.slice_in_dim(result, at, at + a.shape[along], axis=along))
        at += a.shape[along]
    return tuple(done)


def shifted(value, axis, steps):
    count = lax.axis_size(axis)
    leading, last = (max(0, -steps), min(count, count - steps))
    return lax.ppermute(value, axis, [(source, source + steps) for source in range(leading, last)])


def normed(values, gain):
    widened = values.astype(jnp.float32)
    return widened * lax.rsqrt(jnp.mean(widened * widened, axis=-1, keepdims=True) + 1e-06) * gain


def project_rows(rows_here, weights):
    shard_rows = lax.all_gather(rows_here, "tp", axis=0, tiled=True)
    products = [
        jnp.dot(shard_rows, weight, preferred_element_type=jnp.float32).astype(jnp.bfloat16)
        for weight in weights
    ]
    return jnp.concatenate(products, axis=1)


def summed_rows(parts, weight):
    return sent_and_summed(
        jnp.dot(parts, weight, preferred_element_type=jnp.float32).astype(jnp.bfloat16), "tp", 0
    )


def key_columns(source_rows, keyval_first, keyval_second):
    both_layers = jnp.concatenate([keyval_first, keyval_second], axis=1)
    columns = jnp.einsum(
        "rd,dc->cr",
        lax.all_gather(source_rows, "tp", axis=0, tiled=True),
        both_layers,
        preferred_element_type=jnp.float32,
    ).astype(jnp.bfloat16)
    column_count = keyval_first.shape[1]
    stacked = columns.reshape(2, column_count, columns.shape[1])
    own_index = lax.axis_index("tp")
    doublings = (2 * HEAD // column_count).bit_length() - 1
    for bit_number in range(doublings):
        lower_half = own_index // 2**bit_number % 2 == 0
        half_rows = stacked.shape[2] // 2
        outgoing = jnp.where(lower_half, stacked[:, :, half_rows:], stacked[:, :, :half_rows])
        retained = jnp.where(lower_half, stacked[:, :, :half_rows], stacked[:, :, half_rows:])
        partner = swapped(outgoing, "tp", bit_number)
        stacked = jnp.where(
            lower_half,
            jnp.concatenate([retained, partner], axis=1),
            jnp.concatenate([partner, retained], axis=1),
        )
    return (stacked[:, :HEAD], stacked[:, HEAD:])


def absorber(query_heads, running, shard_pair):
    scale_factor = HEAD ** (-0.5)
    best_score, weight_sum, weighted = running
    key_block, value_block = shard_pair
    scores = (
        jnp.einsum("thd,ds->ths", query_heads, key_block, preferred_element_type=jnp.float32)
        * scale_factor
    )
    newest = jnp.max(scores, axis=2)
    rescale = jnp.exp(best_score - newest)
    weights = jnp.exp(scores - newest[:, :, None])
    weight_sum = weight_sum * rescale + jnp.sum(weights, axis=2)
    weighted = weighted * rescale[:, :, None] + jnp.einsum(
        "ths,ds->thd", weights.astype(jnp.bfloat16), value_block, preferred_element_type=jnp.float32
    )
    return (newest, weight_sum, weighted)


def empty_running(row_count, head_count):
    return (
        jnp.full((row_count, head_count), -jnp.inf, jnp.float32),
        jnp.zeros((row_count, head_count), jnp.float32),
        jnp.zeros((row_count, head_count, HEAD), jnp.float32),
    )


def attend_shares(queries, keys_t, values_t):
    row_count = queries.shape[0]
    own_heads = queries.shape[1] // HEAD
    group_count = lax.axis_size("tp") // KVH
    doublings = group_count.bit_length() - 1
    own_index = lax.axis_index("tp")
    grouped = queries
    for bit_number in range(doublings):
        lower_half = own_index // 2**bit_number % 2 == 0
        partner = swapped(grouped, "tp", bit_number)
        grouped = jnp.where(
            lower_half,
            jnp.concatenate([grouped, partner], axis=1),
            jnp.concatenate([partner, grouped], axis=1),
        )
    head_count = grouped.shape[1] // HEAD
    query_heads = grouped.reshape(row_count, head_count, HEAD)
    best_score, weight_sum, weighted = absorber(
        query_heads,
        empty_running(row_count, head_count),
        in_one_piece((keys_t, values_t), "sp", 1, 0),
    )
    for bit_number in range(doublings):
        other_best, other_sum, other_weighted = (
            swapped(best_score.astype(jnp.bfloat16), "tp", bit_number).astype(best_score.dtype),
            swapped(weight_sum.astype(jnp.bfloat16), "tp", bit_number).astype(weight_sum.dtype),
            swapped(weighted.astype(jnp.bfloat16), "tp", bit_number).astype(weighted.dtype),
        )
        newest = jnp.maximum(best_score, other_best)
        own_scale = jnp.exp(best_score - newest)
        other_scale = jnp.exp(other_best - newest)
        weight_sum = weight_sum * own_scale + other_sum * other_scale
        weighted = weighted * own_scale[:, :, None] + other_weighted * other_scale[:, :, None]
        best_score = newest
    first_head = own_index % group_count * own_heads
    chosen = lax.dynamic_slice_in_dim(weighted, first_head, own_heads, 1)
    chosen_sums = lax.dynamic_slice_in_dim(weight_sum, first_head, own_heads, 1)
    return (
        (chosen / chosen_sums[:, :, None]).reshape(row_count, own_heads * HEAD).astype(jnp.bfloat16)
    )


def causal_mix(rim_rows, up_rows, conv_taps):
    padded = jnp.concatenate([rim_rows, up_rows], axis=0).astype(jnp.float32)
    length = up_rows.shape[0]
    return (
        conv_taps[0] * padded[:length]
        + conv_taps[1] * padded[1 : length + 1]
        + conv_taps[2] * padded[2:]
    )


def per_device(
    target,
    source,
    source_gain,
    pre_first,
    query_first,
    keyval_first,
    out_first,
    post_first,
    ffn_pre,
    w_gate,
    w_value,
    conv_gate,
    conv_value,
    w_down,
    ffn_post,
    pre_second,
    query_second,
    keyval_second,
    out_second,
    post_second,
):
    source_rows = normed(source, source_gain).astype(jnp.bfloat16)
    keys_t, values_t = key_columns(source_rows, keyval_first, keyval_second)

    def attention_layer(stream, pre_gain, w_query, layer_index, w_out, post_gain):
        queries = project_rows(normed(stream, pre_gain).astype(jnp.bfloat16), (w_query,))
        heads = attend_shares(queries, keys_t[layer_index], values_t[layer_index])
        mixed = summed_rows(heads, w_out)
        return stream.astype(jnp.float32) + normed(mixed, post_gain)

    after_first = attention_layer(target, pre_first, query_first, 0, out_first, post_first)
    up_both = project_rows(normed(after_first, ffn_pre).astype(jnp.bfloat16), (w_gate, w_value))
    hidden_width = w_gate.shape[1]
    up_gate = up_both[:, :hidden_width]
    up_value = up_both[:, hidden_width:]
    rim_gate, rim_value = shifted((up_gate[-2:], up_value[-2:]), "sp", 1)
    gated = (
        jax.nn.gelu(causal_mix(rim_gate, up_gate, conv_gate), approximate=True)
        * causal_mix(rim_value, up_value, conv_value)
    ).astype(jnp.bfloat16)
    ffn_sum = summed_rows(gated, w_down)
    after_ffn = after_first + normed(ffn_sum, ffn_post)
    return attention_layer(after_ffn, pre_second, query_second, 1, out_second, post_second)


def solution(mesh):
    placed = (
        P(("grp", "sp", "tp"), None),
        P(("grp", "sp", "tp"), None),
        P(),
        P(),
        P(None, "tp"),
        P(None, "tp"),
        P("tp", None),
        P(),
        P(),
        P(None, "tp"),
        P(None, "tp"),
        P(None, "tp"),
        P(None, "tp"),
        P("tp", None),
        P(),
        P(),
        P(None, "tp"),
        P(None, "tp"),
        P("tp", None),
        P(),
    )
    return jax.shard_map(
        per_device,
        mesh=mesh,
        in_specs=placed,
        out_specs=P(("grp", "sp", "tp"), None),
        check_vma=False,
    )
```

profile of v0, /device:TPU:65, one launch (start us, length us, event | category | flops | bytes accessed | tf_op | source)
XLA Modules:
  0.0 380.8 jit_solution(5917875736320434852)
XLA Ops:
  6.6 1.2 fusion.19
  7.8 1.8 fusion.21
  9.8 83.2 %all-gather.4.cloned.1.call-done = bf16[1024,2048]{1,0:T(8,128)(2,1)} async-done(((bf16[64,2048]{1,0:T(8,128)(2,1)}), bf16[1024,2048]{1,0:T(8,128)(2,1)}) %all-gather.4.cloned.1.call-update) | async-done | bytes 4194320 | tf_op jit(solution)/shard_map/all_gather | solution.py:70
  93.0 3.9 %convolution_convert_fusion.3 = bf16[128,1024]{1,0:T(8,128)(2,1)S(1)} fusion(bf16[1024,2048]{1,0:T(8,128)(2,1)} %all-gather.4.cloned.1.call-done, bf16[2048,64]{0,1:T(8,128)(2,1)} %param.37, bf16[2048,64]{0,1:T(8,128)(2,1)} %param.25), kind=kOutput, calls=%fused_computation.16 | convolution fusion | flops 538050560 | bytes 4980736 | tf_op jit(solution)/shard_map/rd,dc->cr/dot_general | solution.py:68
  96.9 2.2 collective-permute-start.2
  100.2 3.0 collective-permute-start.3
  103.3 3.7 collective-permute-done.3
  108.7 18.7 %all_gather.18 = bf16[128,2048]{1,0:T(8,128)(2,1)S(1)} all-gather(bf16[8,2048]{1,0:T(8,128)(2,1)S(1)} %fusion.52), channel_id=1, replica_groups=mesh['grp'=2,'sp'=16,'tp'=16] {'tp'}, dimensions={0}, use_global_device_ids=true | all-gather | bytes 557056 | tf_op jit(solution)/shard_map/all_gather | solution.py:52
  127.7 2.1 collective-permute-start
  130.9 2.0 collective-permute-start.1
  132.8 3.5 collective-permute-done.1
  136.4 41.9 %all-gather.6.cloned.1.call-done = bf16[256,4096]{1,0:T(8,128)(2,1)} async-done(((bf16[256,256]{1,0:T(8,128)(2,1)}), bf16[256,4096]{1,0:T(8,128)(2,1)}) %all-gather.6.cloned.1.call-update) | async-done | bytes 2097168 | tf_op jit(solution)/shard_map/all_gather | solution.py:33
  178.3 2.7 multiply_reduce_fusion.1
  181.1 1.5 fusion
  182.7 13.7 %collective-permute-start.4 = (bf16[128,4]{0,1:T(4,128)(2,1)S(1)}, bf16[128,4]{0,1:T(4,128)(2,1)S(1)}, u32[]{:S(2)}, u32[]{:S(2)}) collective-permute-start(bf16[128,4]{0,1:T(4,128)(2,1)S(1)} %get-tuple-element.43), channel_id=1, source_target_pairs={{0,1},{1,0},{2,3},{3,2},{4,5},{5,4},{6,7},{7,6},{8,9},{9,8},{10,11... | collective-permute-start | bytes 3080 | tf_op jit(solution)/shard_map/ppermute | solution.py:28
  196.4 2.0 collective-permute-start.8
  198.4 3.5 collective-permute-start.6
  201.9 2.0 collective-permute-start.9
  203.9 2.4 collective-permute-done.9
  206.8 2.3 fusion.109
  209.2 4.0 %collective-permute-start.5 = (bf16[128,4,128]{2,0,1:T(8,128)(2,1)}, bf16[128,4,128]{2,0,1:T(8,128)(2,1)}, u32[]{:S(2)}, u32[]{:S(2)}) collective-permute-start(bf16[128,4,128]{2,0,1:T(8,128)(2,1)} %get-tuple-element.47), channel_id=1, source_target_pairs={{0,1},{1,0},{2,3},{3,2},{4,5},{5,4},{6,7},{7,6},{8,9},{9,8},{10,11... | collective-permute-start | bytes 393224 | tf_op jit(solution)/shard_map/ppermute | solution.py:28
  213.2 1.3 collective-permute-done.5
  215.6 2.0 collective-permute-start.7
  218.2 4.0 %collective-permute-done.7 = bf16[128,4,128]{2,0,1:T(8,128)(2,1)S(1)} collective-permute-done((bf16[128,4,128]{2,0,1:T(8,128)(2,1)S(1)}, bf16[128,4,128]{2,0,1:T(8,128)(2,1)S(1)}, u32[]{:S(2)}, u32[]{:S(2)}) %collective-permute-start.7) | collective-permute-done | bytes 131104 | tf_op jit(solution)/shard_map/ppermute | solution.py:28
  222.2 1.2 fusion.8
  223.4 6.5 %all-to-all-start = ((bf16[16,8,2048]{2,1,0:T(8,128)(2,1)}), bf16[16,8,2048]{2,1,0:T(8,128)(2,1)S(1)}, u32[]{:S(2)}, u32[]{:S(2)}) async-start(bf16[16,8,2048]{2,1,0:T(8,128)(2,1)} %fusion.8), calls=%async_computation | async-start | bytes 1048576 | tf_op jit(solution)/shard_map/all_to_all | solution.py:17
  231.6 1.5 pad_maximum_fusion.1
  233.2 13.9 %all-to-all-done = bf16[16,8,2048]{2,1,0:T(8,128)(2,1)S(1)} async-done(((bf16[16,8,2048]{2,1,0:T(8,128)(2,1)}), bf16[16,8,2048]{2,1,0:T(8,128)(2,1)S(1)}, u32[]{:S(2)}, u32[]{:S(2)}) %all-to-all-start) | async-done | bytes 524320 | tf_op jit(solution)/shard_map/all_to_all | solution.py:17
  247.6 16.0 %all_gather.21 = bf16[128,2048]{1,0:T(8,128)(2,1)S(1)} all-gather(bf16[8,2048]{1,0:T(8,128)(2,1)S(1)} %multiply_convert_fusion.1), channel_id=1, replica_groups=mesh['grp'=2,'sp'=16,'tp'=16] {'tp'}, dimensions={0}, use_global_device_ids=true | all-gather | bytes 557056 | tf_op jit(solution)/shard_map/all_gather | solution.py:52
  264.1 3.2 collective-permute-start.10
  267.8 2.1 collective-permute-start.11
  271.7 23.3 %all_to_all.15 = bf16[16,8,2048]{2,1,0:T(8,128)(2,1)S(1)} all-to-all(bf16[16,8,2048]{2,1,0:T(8,128)(2,1)S(1)} %fusion.9), channel_id=1, replica_groups=mesh['grp'=2,'sp'=16,'tp'=16] {'tp'}, dimensions={0} | all-to-all | bytes 1048576 | tf_op jit(solution)/shard_map/all_to_all | solution.py:17
  295.6 16.0 %all_gather.22 = bf16[128,2048]{1,0:T(8,128)(2,1)S(1)} all-gather(bf16[8,2048]{1,0:T(8,128)(2,1)S(1)} %multiply_convert_fusion), channel_id=1, replica_groups=mesh['grp'=2,'sp'=16,'tp'=16] {'tp'}, dimensions={0}, use_global_device_ids=true | all-gather | bytes 557056 | tf_op jit(solution)/shard_map/all_gather | solution.py:52
  311.9 2.1 collective-permute-start.12
  315.1 2.2 collective-permute-start.13
  317.3 3.2 collective-permute-done.13
  320.5 2.7 multiply_reduce_fusion
  323.2 1.5 fusion.2
  324.7 3.0 collective-permute-start.14
  327.7 2.0 collective-permute-start.18
  329.7 2.2 collective-permute-start.16
  331.9 3.2 collective-permute-start.19
  335.1 1.2 collective-permute-done.19
  336.3 1.7 fusion.110
  338.0 3.9 %collective-permute-start.15 = (bf16[128,4,128]{2,0,1:T(8,128)(2,1)S(1)}, bf16[128,4,128]{2,0,1:T(8,128)(2,1)S(1)}, u32[]{:S(2)}, u32[]{:S(2)}) collective-permute-start(bf16[128,4,128]{2,0,1:T(8,128)(2,1)S(1)} %get-tuple-element.51), channel_id=1, source_target_pairs={{0,1},{1,0},{2,3},{3,2},{4,5},{5,4},{6,7},{7,6},{8,9},{9,8},{10,11... | collective-permute-start | bytes 393224 | tf_op jit(solution)/shard_map/ppermute | solution.py:28
  343.0 3.2 collective-permute-start.17
  346.2 3.4 collective-permute-done.17
  350.0 23.3 %all_to_all.16 = bf16[16,8,2048]{2,1,0:T(8,128)(2,1)S(1)} all-to-all(bf16[16,8,2048]{2,1,0:T(8,128)(2,1)S(1)} %fusion.10), channel_id=1, replica_groups=mesh['grp'=2,'sp'=16,'tp'=16] {'tp'}, dimensions={0} | all-to-all | bytes 1048576 | tf_op jit(solution)/shard_map/all_to_all | solution.py:17
  (108 shorter events, 16.3 us)
Async XLA Ops:
  6.5 264.6 %copy-start = (bf16[176,2048]{1,0:T(8,128)(2,1)S(1)}, bf16[176,2048]{1,0:T(8,128)(2,1)}, u32[]{:S(2)}) copy-start(bf16[176,2048]{1,0:T(8,128)(2,1)} %param.33) | copy-start | bytes 2162692
  6.6 101.9 %copy-start.1 = (bf16[8,2048]{1,0:T(8,128)(2,1)S(1)}, bf16[8,2048]{1,0:T(8,128)(2,1)}, u32[]{:S(2)}) copy-start(bf16[8,2048]{1,0:T(8,128)(2,1)} %param.20) | copy-start | bytes 98308
  6.6 102.0 %copy-start.11 = (f32[2048]{0:T(1024)S(1)}, f32[2048]{0:T(1024)}, u32[]{:S(2)}) copy-start(f32[2048]{0:T(1024)} %param.23) | copy-start | bytes 24580
  6.6 120.8 %copy-start.4 = (bf16[2048,128]{1,0:T(8,128)(2,1)S(1)}, bf16[2048,128]{1,0:T(8,128)(2,1)}, u32[]{:S(2)}) copy-start(bf16[2048,128]{1,0:T(8,128)(2,1)} %param.24) | copy-start | bytes 1572868
  6.6 86.4 %all-gather.4.cloned.1.call-start = ((), (), s32[]{:S(2)}) async-start(), calls=%async_computation.3 | async-start | bytes 4456448 | tf_op jit(solution)/shard_map/all_gather | solution.py:70
  9.7 168.6 %all-gather.6.cloned.1.call-start = ((), (), s32[]{:S(2)}) async-start(), calls=%async_computation.4 | async-start | bytes 2228224 | tf_op jit(solution)/shard_map/all_gather | solution.py:33
  96.9 3.3 collective-permute-start.2
  100.2 6.7 %collective-permute-start.3 = (bf16[2,128,256]{2,1,0:T(8,128)(2,1)S(1)}, bf16[2,128,256]{2,1,0:T(8,128)(2,1)S(1)}, u32[]{:S(2)}, u32[]{:S(2)}) collective-permute-start(bf16[2,128,256]{2,1,0:T(8,128)(2,1)S(1)} %get-tuple-element.30), channel_id=1, source_target_pairs={{0,2},{2,0},{1,3},{3,1},{4,6},{6,4},{5,7},{7,5},{8,10},{10,8},{9,1... | collective-permute-start | bytes 393224 | tf_op jit(solution)/shard_map/ppermute | solution.py:28
  127.7 3.1 collective-permute-start
  130.9 5.5 %collective-permute-start.1 = (bf16[128,256]{0,1:T(8,128)(2,1)S(1)}, bf16[128,256]{0,1:T(8,128)(2,1)S(1)}, u32[]{:S(2)}, u32[]{:S(2)}) collective-permute-start(bf16[128,256]{0,1:T(8,128)(2,1)S(1)} %maximum_select_fusion.7), channel_id=1, source_target_pairs={{0,2},{2,0},{1,3},{3,1},{4,6},{6,4},{5,7},{7,5},{8,10},{10,8},{9,1... | collective-permute-start | bytes 196616 | tf_op jit(solution)/shard_map/ppermute | solution.py:28
  178.3 28.5 %copy-start.9 = (bf16[256,4096]{1,0:T(8,128)(2,1)S(1)}, bf16[256,4096]{1,0:T(8,128)(2,1)}, u32[]{:S(2)}) copy-start(bf16[256,4096]{1,0:T(8,128)(2,1)} %all-gather.6.cloned.1.call-done) | copy-start | bytes 6291460
  181.1 41.1 %copy-start.5 = (bf16[128,2048]{1,0:T(8,128)(2,1)S(1)}, bf16[128,2048]{1,0:T(8,128)(2,1)}, u32[]{:S(2)}) copy-start(bf16[128,2048]{1,0:T(8,128)(2,1)} %param.26) | copy-start | bytes 1572868
  182.6 64.7 %copy-start.10 = (f32[2048]{0:T(1024)S(1)}, f32[2048]{0:T(1024)}, u32[]{:S(2)}) copy-start(f32[2048]{0:T(1024)} %param.27) | copy-start | bytes 24580
  182.6 64.9 %copy-start.12 = (f32[2048]{0:T(1024)S(1)}, f32[2048]{0:T(1024)}, u32[]{:S(2)}) copy-start(f32[2048]{0:T(1024)} %param.28) | copy-start | bytes 24580
  182.6 81.0 %copy-start.2 = (bf16[2048,176]{0,1:T(8,128)(2,1)S(1)}, bf16[2048,176]{0,1:T(8,128)(2,1)}, u32[]{:S(2)}) copy-start(bf16[2048,176]{0,1:T(8,128)(2,1)} %param.29) | copy-start | bytes 2162692
  182.6 84.7 %copy-start.3 = (bf16[2048,176]{0,1:T(8,128)(2,1)S(1)}, bf16[2048,176]{0,1:T(8,128)(2,1)}, u32[]{:S(2)}) copy-start(bf16[2048,176]{0,1:T(8,128)(2,1)} %param.30) | copy-start | bytes 2162692
  182.7 15.7 %collective-permute-start.4 = (bf16[128,4]{0,1:T(4,128)(2,1)S(1)}, bf16[128,4]{0,1:T(4,128)(2,1)S(1)}, u32[]{:S(2)}, u32[]{:S(2)}) collective-permute-start(bf16[128,4]{0,1:T(4,128)(2,1)S(1)} %get-tuple-element.43), channel_id=1, source_target_pairs={{0,1},{1,0},{2,3},{3,2},{4,5},{5,4},{6,7},{7,6},{8,9},{9,8},{10,11... | collective-permute-start | bytes 3080 | tf_op jit(solution)/shard_map/ppermute | solution.py:28
  196.4 5.5 %collective-permute-start.8 = (bf16[128,4]{0,1:T(4,128)(2,1)S(1)}, bf16[128,4]{0,1:T(4,128)(2,1)S(1)}, u32[]{:S(2)}, u32[]{:S(2)}) collective-permute-start(bf16[128,4]{0,1:T(4,128)(2,1)S(1)} %get-tuple-element.44), channel_id=1, source_target_pairs={{0,1},{1,0},{2,3},{3,2},{4,5},{5,4},{6,7},{7,6},{8,9},{9,8},{10,11... | collective-permute-start | bytes 3080 | tf_op jit(solution)/shard_map/ppermute | solution.py:28
  198.4 5.5 %collective-permute-start.6 = (bf16[128,4]{0,1:T(4,128)(2,1)S(1)}, bf16[128,4]{0,1:T(4,128)(2,1)S(1)}, u32[]{:S(2)}, u32[]{:S(2)}) collective-permute-start(bf16[128,4]{0,1:T(4,128)(2,1)S(1)} %fusion.82), channel_id=1, source_target_pairs={{0,2},{2,0},{1,3},{3,1},{4,6},{6,4},{5,7},{7,5},{8,10},{10,8},{9,1... | collective-permute-start | bytes 3080 | tf_op jit(solution)/shard_map/ppermute | solution.py:28
  201.9 4.3 %collective-permute-start.9 = (bf16[128,4]{0,1:T(4,128)(2,1)S(1)}, bf16[128,4]{0,1:T(4,128)(2,1)S(1)}, u32[]{:S(2)}, u32[]{:S(2)}) collective-permute-start(bf16[128,4]{0,1:T(4,128)(2,1)S(1)} %get-tuple-element.19), channel_id=1, source_target_pairs={{0,2},{2,0},{1,3},{3,1},{4,6},{6,4},{5,7},{7,5},{8,10},{10,8},{9,1... | collective-permute-start | bytes 3080 | tf_op jit(solution)/shard_map/ppermute | solution.py:28
  206.8 88.4 %copy-start.13 = (f32[2048]{0:T(1024)S(1)}, f32[2048]{0:T(1024)}, u32[]{:S(2)}) copy-start(f32[2048]{0:T(1024)} %param.34) | copy-start | bytes 24580
  206.8 88.7 %copy-start.15 = (f32[2048]{0:T(1024)S(1)}, f32[2048]{0:T(1024)}, u32[]{:S(2)}) copy-start(f32[2048]{0:T(1024)} %param.35) | copy-start | bytes 24580
  209.2 102.4 %copy-start.6 = (bf16[2048,128]{1,0:T(8,128)(2,1)S(1)}, bf16[2048,128]{1,0:T(8,128)(2,1)}, u32[]{:S(2)}) copy-start(bf16[2048,128]{1,0:T(8,128)(2,1)} %param.36) | copy-start | bytes 1572868
  209.2 5.3 %collective-permute-start.5 = (bf16[128,4,128]{2,0,1:T(8,128)(2,1)}, bf16[128,4,128]{2,0,1:T(8,128)(2,1)}, u32[]{:S(2)}, u32[]{:S(2)}) collective-permute-start(bf16[128,4,128]{2,0,1:T(8,128)(2,1)} %get-tuple-element.47), channel_id=1, source_target_pairs={{0,1},{1,0},{2,3},{3,2},{4,5},{5,4},{6,7},{7,6},{8,9},{9,8},{10,11... | collective-permute-start | bytes 393224 | tf_op jit(solution)/shard_map/ppermute | solution.py:28
  215.6 6.6 %collective-permute-start.7 = (bf16[128,4,128]{2,0,1:T(8,128)(2,1)S(1)}, bf16[128,4,128]{2,0,1:T(8,128)(2,1)S(1)}, u32[]{:S(2)}, u32[]{:S(2)}) collective-permute-start(bf16[128,4,128]{2,0,1:T(8,128)(2,1)S(1)} %get-tuple-element.23), channel_id=1, source_target_pairs={{0,2},{2,0},{1,3},{3,1},{4,6},{6,4},{5,7},{7,5},{8,10},{10,8},{9,1... | collective-permute-start | bytes 393224 | tf_op jit(solution)/shard_map/ppermute | solution.py:28
  223.4 23.7 %all-to-all-start = ((bf16[16,8,2048]{2,1,0:T(8,128)(2,1)}), bf16[16,8,2048]{2,1,0:T(8,128)(2,1)S(1)}, u32[]{:S(2)}, u32[]{:S(2)}) async-start(bf16[16,8,2048]{2,1,0:T(8,128)(2,1)} %fusion.8), calls=%async_computation | async-start | bytes 1048576 | tf_op jit(solution)/shard_map/all_to_all | solution.py:17
  229.9 87.4 %all-gather.8.cloned.1.call-start = ((), (), s32[]{:S(2)}) async-start(), calls=%async_computation.5 | async-start | bytes 2228224 | tf_op jit(solution)/shard_map/all_gather | solution.py:33
  264.1 5.8 %collective-permute-start.10 = (bf16[2,176]{0,1:T(8,128)(2,1)S(1)}, bf16[2,176]{0,1:T(8,128)(2,1)S(1)}, u32[]{:S(2)}, u32[]{:S(2)}) collective-permute-start(bf16[2,176]{0,1:T(8,128)(2,1)S(1)} %slice.122), channel_id=1, source_target_pairs={{0,16},{16,32},{32,48},{48,64},{64,80},{80,96},{96,112},{112,128},... | collective-permute-start | bytes 2120 | tf_op jit(solution)/shard_map/ppermute | solution.py:43
  267.8 3.2 collective-permute-start.11
  311.9 3.1 collective-permute-start.12
  315.1 5.4 %collective-permute-start.13 = (bf16[128,256]{0,1:T(8,128)(2,1)S(1)}, bf16[128,256]{0,1:T(8,128)(2,1)S(1)}, u32[]{:S(2)}, u32[]{:S(2)}) collective-permute-start(bf16[128,256]{0,1:T(8,128)(2,1)S(1)} %maximum_select_fusion.9), channel_id=1, source_target_pairs={{0,2},{2,0},{1,3},{3,1},{4,6},{6,4},{5,7},{7,5},{8,10},{10,8},{9,1... | collective-permute-start | bytes 196616 | tf_op jit(solution)/shard_map/ppermute | solution.py:28
  320.5 15.8 %copy-start.8 = (bf16[256,4096]{1,0:T(8,128)(2,1)S(1)}, bf16[256,4096]{1,0:T(8,128)(2,1)}, u32[]{:S(2)}) copy-start(bf16[256,4096]{1,0:T(8,128)(2,1)} %all-gather.8.cloned.1.call-done) | copy-start | bytes 6291460
  323.2 26.4 %copy-start.7 = (bf16[128,2048]{1,0:T(8,128)(2,1)S(1)}, bf16[128,2048]{1,0:T(8,128)(2,1)}, u32[]{:S(2)}) copy-start(bf16[128,2048]{1,0:T(8,128)(2,1)} %param.38) | copy-start | bytes 1572868
  324.7 48.8 %copy-start.14 = (f32[2048]{0:T(1024)S(1)}, f32[2048]{0:T(1024)}, u32[]{:S(2)}) copy-start(f32[2048]{0:T(1024)} %param.39) | copy-start | bytes 24580
  324.7 4.9 %collective-permute-start.14 = (bf16[128,4]{0,1:T(4,128)(2,1)S(1)}, bf16[128,4]{0,1:T(4,128)(2,1)S(1)}, u32[]{:S(2)}, u32[]{:S(2)}) collective-permute-start(bf16[128,4]{0,1:T(4,128)(2,1)S(1)} %get-tuple-element.40), channel_id=1, source_target_pairs={{0,1},{1,0},{2,3},{3,2},{4,5},{5,4},{6,7},{7,6},{8,9},{9,8},{10,11... | collective-permute-start | bytes 3080 | tf_op jit(solution)/shard_map/ppermute | solution.py:28
  327.7 4.2 %collective-permute-start.18 = (bf16[128,4]{0,1:T(4,128)(2,1)S(1)}, bf16[128,4]{0,1:T(4,128)(2,1)S(1)}, u32[]{:S(2)}, u32[]{:S(2)}) collective-permute-start(bf16[128,4]{0,1:T(4,128)(2,1)S(1)} %get-tuple-element.41), channel_id=1, source_target_pairs={{0,1},{1,0},{2,3},{3,2},{4,5},{5,4},{6,7},{7,6},{8,9},{9,8},{10,11... | collective-permute-start | bytes 3080 | tf_op jit(solution)/shard_map/ppermute | solution.py:28
  329.7 5.4 %collective-permute-start.16 = (bf16[128,4]{0,1:T(4,128)(2,1)S(1)}, bf16[128,4]{0,1:T(4,128)(2,1)S(1)}, u32[]{:S(2)}, u32[]{:S(2)}) collective-permute-start(bf16[128,4]{0,1:T(4,128)(2,1)S(1)} %fusion.83), channel_id=1, source_target_pairs={{0,2},{2,0},{1,3},{3,1},{4,6},{6,4},{5,7},{7,5},{8,10},{10,8},{9,1... | collective-permute-start | bytes 3080 | tf_op jit(solution)/shard_map/ppermute | solution.py:28
  331.9 4.3 %collective-permute-start.19 = (bf16[128,4]{0,1:T(4,128)(2,1)S(1)}, bf16[128,4]{0,1:T(4,128)(2,1)S(1)}, u32[]{:S(2)}, u32[]{:S(2)}) collective-permute-start(bf16[128,4]{0,1:T(4,128)(2,1)S(1)} %get-tuple-element.8), channel_id=1, source_target_pairs={{0,2},{2,0},{1,3},{3,1},{4,6},{6,4},{5,7},{7,5},{8,10},{10,8},{9,1... | collective-permute-start | bytes 3080 | tf_op jit(solution)/shard_map/ppermute | solution.py:28
  338.0 4.8 %collective-permute-start.15 = (bf16[128,4,128]{2,0,1:T(8,128)(2,1)S(1)}, bf16[128,4,128]{2,0,1:T(8,128)(2,1)S(1)}, u32[]{:S(2)}, u32[]{:S(2)}) collective-permute-start(bf16[128,4,128]{2,0,1:T(8,128)(2,1)S(1)} %get-tuple-element.51), channel_id=1, source_target_pairs={{0,1},{1,0},{2,3},{3,2},{4,5},{5,4},{6,7},{7,6},{8,9},{9,8},{10,11... | collective-permute-start | bytes 393224 | tf_op jit(solution)/shard_map/ppermute | solution.py:28
  343.0 6.6 %collective-permute-start.17 = (bf16[128,4,128]{2,0,1:T(8,128)(2,1)S(1)}, bf16[128,4,128]{2,0,1:T(8,128)(2,1)S(1)}, u32[]{:S(2)}, u32[]{:S(2)}) collective-permute-start(bf16[128,4,128]{2,0,1:T(8,128)(2,1)S(1)} %get-tuple-element.12), channel_id=1, source_target_pairs={{0,2},{2,0},{1,3},{3,1},{4,6},{6,4},{5,7},{7,5},{8,10},{10,8},{9,1... | collective-permute-start | bytes 393224 | tf_op jit(solution)/shard_map/ppermute | solution.py:28
Sparse Core Ops, SparseCore 0:
  9.8 83.0 all-gather.3
  108.6 69.7 all-gather.5
  233.3 66.6 all-gather.7
where the time goes:
time: 382 us; the launch traced here: 381 us
  waiting for transfers between devices  167 us (44%)
  blocking collectives  97.2 us (25%)
  starting transfers between devices  70 us (18%)
  matrix products  16.9 us (4%)
  between operations  13.8 us (4%)
  other arithmetic  12.8 us (3%)
    all_gather x1, waiting for transfers between devices, key_columns(): lax.all_gather(source_rows, 'tp', axis=0, tiled=True)  83.2 us
    ppermute x18, starting transfers between devices, swapped(): return lax.ppermute(block, axis, route)  57.9 us
    all_gather x3, blocking collectives, project_rows(): shard_rows = lax.all_gather(rows_here, 'tp', axis=0, tiled=True)  50.6 us
    all_to_all x2, blocking collectives, sent_and_summed(): lax.all_to_all(parts, axis, split_axis=0, concat_axis=0, tiled=True)  46.6 us
    all_gather x2, waiting for transfers between devices, in_one_piece(): result, at, done = (lax.all_gather(both, axis, axis=dim, tiled=True), 0, [])  42 us
    ppermute x18, waiting for transfers between devices, swapped(): return lax.ppermute(block, axis, route)  26.6 us
    all_to_all x1, waiting for transfers between devices, sent_and_summed(): lax.all_to_all(parts, axis, split_axis=0, concat_axis=0, tiled=True)  13.9 us
  transfers between devices with their start and end apart: 24, of which 16 were waited for; matrix products, arithmetic and copies ran while one was open for 2% of the time, Pallas kernels for 0%

commit v1 on v0

--- a/solution.py
+++ b/solution.py
@@ -5,6 +5,27 @@
 
 HEAD = 128
 KVH = 4
+
+
+def gather_around(array, axis, dim):
+    peers, index, rows = (lax.axis_size(axis), lax.axis_index(axis), array.shape[dim])
+    right = [(i, (i + 1) % peers) for i in range(peers)]
+    behind = [(i, (i - 1) % peers) for i in range(peers)]
+    filled = jnp.zeros((*array.shape[:dim], peers * rows, *array.shape[dim + 1 :]), array.dtype)
+    filled = lax.dynamic_update_slice_in_dim(filled, array, index * rows, axis=dim)
+    from_left = from_right = array
+    middle = peers // 2
+    for hop in range(1, middle + 1):
+        from_left = lax.ppermute(from_left, axis, right)
+        filled = lax.dynamic_update_slice_in_dim(
+            filled, from_left, (index - hop) % peers * rows, axis=dim
+        )
+        if hop < peers - middle:
+            from_right = lax.ppermute(from_right, axis, behind)
+            filled = lax.dynamic_update_slice_in_dim(
+                filled, from_right, (index + hop) % peers * rows, axis=dim
+            )
+    return filled
 
 
 def in_blocks(array, dim, size):
@@ -49,7 +70,7 @@
 
 
 def project_rows(rows_here, weights):
-    shard_rows = lax.all_gather(rows_here, "tp", axis=0, tiled=True)
+    shard_rows = gather_around(rows_here, "tp", 0)
     products = [
         jnp.dot(shard_rows, weight, preferred_element_type=jnp.float32).astype(jnp.bfloat16)
         for weight in weights

time: 382 us -> 441 us (1.15)
  starting transfers between devices: 70 us -> 164 us
  blocking collectives: 97.2 us -> 24.1 us
  waiting for transfers between devices: 167 us -> 207 us
    ppermute x0 -> x45, starting transfers between devices: none -> 65.1 us  [the longest x21 44.9 us: gather_around(): from_right = lax.ppermute(from_right, axis, behind)]
    all_gather x3 -> x0, blocking collectives: 50.6 us -> none  [project_rows(): shard_rows = lax.all_gather(rows_here, 'tp', axis=0, tiled=True)]
    ppermute x0 -> x45, waiting for transfers between devices: none -> 31.1 us  [the longest x24 25.7 us: gather_around(): from_left = lax.ppermute(from_left, axis, right)]
    all_to_all x2 -> x1, blocking collectives: 46.6 us -> 24.1 us  [sent_and_summed(): lax.all_to_all(parts, axis, split_axis=0, concat_axis=0, tiled=True)]
    all_to_all x1 -> x2, waiting for transfers between devices: 13.9 us -> 33.6 us  [sent_and_summed(): lax.all_to_all(parts, axis, split_axis=0, concat_axis=0, tiled=True)]
    ppermute x18, starting transfers between devices: 57.9 us -> 77.4 us  [swapped(): return lax.ppermute(block, axis, route)]
    all_to_all x1 -> x2, starting transfers between devices: 6.52 us -> 16.2 us  [sent_and_summed(): lax.all_to_all(parts, axis, split_axis=0, concat_axis=0, tiled=True)]
    all_gather x2, waiting for transfers between devices: 42 us -> 36.3 us  [in_one_piece(): result, at, done = (lax.all_gather(both, axis, axis=dim, tiled=True), 0, [])]
  transfers between devices with their start and end apart: 24 -> 70, of which waited for: 16 -> 59; matrix products, arithmetic and copies ran while one was open for 2% -> 1% of each run, Pallas kernels for 0% -> 0%
where the time goes in v1:
time: 441 us; the launch traced here: 440 us
  waiting for transfers between devices  207 us (47%)
  starting transfers between devices  164 us (37%)
  blocking collectives  24.1 us (5%)
  matrix products  17.9 us (4%)
  between operations  14 us (3%)
  other arithmetic  12.2 us (3%)
    all_gather x1, waiting for transfers between devices, key_columns(): lax.all_gather(source_rows, 'tp', axis=0, tiled=True)  83.2 us
    ppermute x18, starting transfers between devices, swapped(): return lax.ppermute(block, axis, route)  77.4 us
    ppermute x21, starting transfers between devices, gather_around(): from_right = lax.ppermute(from_right, axis, behind)  44.9 us
    all_gather x2, waiting for transfers between devices, in_one_piece(): result, at, done = (lax.all_gather(both, axis, axis=dim, tiled=True), 0, [])  36.3 us
    all_to_all x2, waiting for transfers between devices, sent_and_summed(): lax.all_to_all(parts, axis, split_axis=0, concat_axis=0, tiled=True)  33.6 us
    ppermute x24, waiting for transfers between devices, gather_around(): from_left = lax.ppermute(from_left, axis, right)  25.7 us
    all_to_all x1, blocking collectives, sent_and_summed(): lax.all_to_all(parts, axis, split_axis=0, concat_axis=0, tiled=True)  24.1 us
    ppermute x18, waiting for transfers between devices, swapped(): return lax.ppermute(block, axis, route)  21.7 us
  transfers between devices with their start and end apart: 70, of which 59 were waited for; matrix products, arithmetic and copies ran while one was open for 1% of the time, Pallas kernels for 0%

profile of v1, /device:TPU:65, one launch (start us, length us, event | category | flops | bytes accessed | tf_op | source)
XLA Modules:
  0.0 440.4 jit_solution(9529758403261810134)
XLA Ops:
  9.8 83.2 %all-gather.4.cloned.1.call-done = bf16[1024,2048]{1,0:T(8,128)(2,1)} async-done(((bf16[64,2048]{1,0:T(8,128)(2,1)}), bf16[1024,2048]{1,0:T(8,128)(2,1)}) %all-gather.4.cloned.1.call-update) | async-done | bytes 4194320 | tf_op jit(solution)/shard_map/all_gather | solution.py:91
  92.9 3.9 convolution_convert_fusion.3
  100.2 3.0 collective-permute-start.18
  103.3 3.6 collective-permute-done.18
  111.1 2.3 collective-permute-start.2
  114.4 2.3 collective-permute-start.4
  120.1 2.7 collective-permute-start.7
  123.6 3.7 collective-permute-start.9
  128.2 3.7 collective-permute-start.11
  132.7 4.1 collective-permute-start.13
  137.7 4.0 collective-permute-done.14
  142.0 5.8 %collective-permute-start.15 = (bf16[128,128]{0,1:T(8,128)(2,1)S(1)}, bf16[128,128]{0,1:T(8,128)(2,1)S(1)}, u32[]{:S(2)}, u32[]{:S(2)}) collective-permute-start(bf16[128,128]{0,1:T(8,128)(2,1)S(1)} %convolution_convert_fusion.7), channel_id=1, source_target_pairs={{0,1},{1,0},{2,3},{3,2},{4,5},{5,4},{6,7},{7,6},{8,9},{9,8},{10,11... | collective-permute-start | bytes 98312 | tf_op jit(solution)/shard_map/ppermute | solution.py:49
  150.6 3.1 collective-permute-done.16
  153.7 24.0 %all-gather.6.cloned.1.call-done = bf16[256,4096]{1,0:T(8,128)(2,1)} async-done(((bf16[256,256]{1,0:T(8,128)(2,1)}), bf16[256,4096]{1,0:T(8,128)(2,1)}) %all-gather.6.cloned.1.call-update) | async-done | bytes 2097168 | tf_op jit(solution)/shard_map/all_gather | solution.py:54
  177.7 2.7 multiply_reduce_fusion.1
  182.0 13.9 %collective-permute-start.19 = (bf16[128,4]{0,1:T(4,128)(2,1)S(1)}, bf16[128,4]{0,1:T(4,128)(2,1)S(1)}, u32[]{:S(2)}, u32[]{:S(2)}) collective-permute-start(bf16[128,4]{0,1:T(4,128)(2,1)S(1)} %get-tuple-element.49), channel_id=1, source_target_pairs={{0,1},{1,0},{2,3},{3,2},{4,5},{5,4},{6,7},{7,6},{8,9},{9,8},{10,11... | collective-permute-start | bytes 3080 | tf_op jit(solution)/shard_map/ppermute | solution.py:49
  197.9 2.8 collective-permute-start.21
  200.8 2.6 collective-permute-start.24
  205.1 2.4 fusion.110
  207.6 4.0 collective-permute-start.20
  214.1 2.6 collective-permute-start.22
  216.7 4.0 collective-permute-done.22
  221.9 7.1 %all-to-all-start = ((bf16[16,8,2048]{2,1,0:T(8,128)(2,1)}), bf16[16,8,2048]{2,1,0:T(8,128)(2,1)S(1)}, u32[]{:S(2)}, u32[]{:S(2)}) async-start(bf16[16,8,2048]{2,1,0:T(8,128)(2,1)} %fusion.8), calls=%async_computation | async-start | bytes 1048576 | tf_op jit(solution)/shard_map/all_to_all | solution.py:38
  229.0 17.2 %all-to-all-done = bf16[16,8,2048]{2,1,0:T(8,128)(2,1)S(1)} async-done(((bf16[16,8,2048]{2,1,0:T(8,128)(2,1)}), bf16[16,8,2048]{2,1,0:T(8,128)(2,1)S(1)}, u32[]{:S(2)}, u32[]{:S(2)}) %all-to-all-start) | async-done | bytes 524320 | tf_op jit(solution)/shard_map/all_to_all | solution.py:38
  251.3 2.3 collective-permute-start.29
  260.6 3.4 collective-permute-start.34
  264.8 3.7 collective-permute-start.36
  269.4 3.7 collective-permute-start.38
  273.9 4.3 collective-permute-done.39
  278.7 3.3 collective-permute-start.40
  287.4 9.1 %all-to-all-start.1 = ((bf16[16,8,2048]{2,1,0:T(8,128)(2,1)}), bf16[16,8,2048]{2,1,0:T(8,128)(2,1)S(1)}, u32[]{:S(2)}, u32[]{:S(2)}) async-start(bf16[16,8,2048]{2,1,0:T(8,128)(2,1)} %fusion.9), calls=%async_computation.1 | async-start | bytes 1048576 | tf_op jit(solution)/shard_map/all_to_all | solution.py:38
  297.3 16.4 %all-to-all-done.1 = bf16[16,8,2048]{2,1,0:T(8,128)(2,1)S(1)} async-done(((bf16[16,8,2048]{2,1,0:T(8,128)(2,1)}), bf16[16,8,2048]{2,1,0:T(8,128)(2,1)S(1)}, u32[]{:S(2)}, u32[]{:S(2)}) %all-to-all-start.1) | async-done | bytes 524320 | tf_op jit(solution)/shard_map/all_to_all | solution.py:38
  318.7 2.3 collective-permute-start.46
  324.7 2.4 collective-permute-start.49
  328.1 3.6 collective-permute-start.51
  332.5 3.7 collective-permute-start.53
  337.1 3.7 collective-permute-start.55
  341.6 4.1 collective-permute-done.56
  346.1 5.8 %collective-permute-start.57 = (bf16[128,128]{0,1:T(8,128)(2,1)S(1)}, bf16[128,128]{0,1:T(8,128)(2,1)S(1)}, u32[]{:S(2)}, u32[]{:S(2)}) collective-permute-start(bf16[128,128]{0,1:T(8,128)(2,1)S(1)} %convolution_convert_fusion.6), channel_id=1, source_target_pairs={{0,1},{1,0},{2,3},{3,2},{4,5},{5,4},{6,7},{7,6},{8,9},{9,8},{10,11... | collective-permute-start | bytes 98312 | tf_op jit(solution)/shard_map/ppermute | solution.py:49
  354.7 12.4 %all-gather.8.cloned.1.call-done = bf16[256,4096]{1,0:T(8,128)(2,1)} async-done(((bf16[256,256]{1,0:T(8,128)(2,1)}), bf16[256,4096]{1,0:T(8,128)(2,1)}) %all-gather.8.cloned.1.call-update) | async-done | bytes 2097168 | tf_op jit(solution)/shard_map/all_gather | solution.py:54
  367.1 2.7 multiply_reduce_fusion
  371.4 14.8 %collective-permute-start.59 = (bf16[128,4]{0,1:T(4,128)(2,1)S(1)}, bf16[128,4]{0,1:T(4,128)(2,1)S(1)}, u32[]{:S(2)}, u32[]{:S(2)}) collective-permute-start(bf16[128,4]{0,1:T(4,128)(2,1)S(1)} %get-tuple-element.46), channel_id=1, source_target_pairs={{0,1},{1,0},{2,3},{3,2},{4,5},{5,4},{6,7},{7,6},{8,9},{9,8},{10,11... | collective-permute-start | bytes 3080 | tf_op jit(solution)/shard_map/ppermute | solution.py:49
  388.2 2.5 collective-permute-start.61
  390.7 2.9 collective-permute-start.64
  396.8 3.9 collective-permute-start.60
  401.8 2.9 collective-permute-start.62
  404.7 3.7 collective-permute-done.62
  408.8 24.1 %all_to_all.15 = bf16[16,8,2048]{2,1,0:T(8,128)(2,1)S(1)} all-to-all(bf16[16,8,2048]{2,1,0:T(8,128)(2,1)S(1)} %fusion.10), channel_id=1, replica_groups=mesh['grp'=2,'sp'=16,'tp'=16] {'tp'}, dimensions={0} | all-to-all | bytes 1048576 | tf_op jit(solution)/shard_map/all_to_all | solution.py:38
  (248 shorter events, 76.1 us)
Async XLA Ops:
  6.6 86.4 %all-gather.4.cloned.1.call-start = ((), (), s32[]{:S(2)}) async-start(), calls=%async_computation.3 | async-start | bytes 4456448 | tf_op jit(solution)/shard_map/all_gather | solution.py:91
  9.7 168.0 %all-gather.6.cloned.1.call-start = ((), (), s32[]{:S(2)}) async-start(), calls=%async_computation.4 | async-start | bytes 2228224 | tf_op jit(solution)/shard_map/all_gather | solution.py:54
  100.2 6.7 %collective-permute-start.18 = (bf16[2,128,256]{2,1,0:T(8,128)(2,1)S(1)}, bf16[2,128,256]{2,1,0:T(8,128)(2,1)S(1)}, u32[]{:S(2)}, u32[]{:S(2)}) collective-permute-start(bf16[2,128,256]{2,1,0:T(8,128)(2,1)S(1)} %get-tuple-element.36), channel_id=1, source_target_pairs={{0,2},{2,0},{1,3},{3,1},{4,6},{6,4},{5,7},{7,5},{8,10},{10,8},{9,1... | collective-permute-start | bytes 393224 | tf_op jit(solution)/shard_map/ppermute | solution.py:49
  114.4 4.5 %collective-permute-start.4 = (bf16[8,2048]{1,0:T(8,128)(2,1)S(1)}, bf16[8,2048]{1,0:T(8,128)(2,1)S(1)}, u32[]{:S(2)}, u32[]{:S(2)}) collective-permute-start(bf16[8,2048]{1,0:T(8,128)(2,1)S(1)} %collective-permute-done.2), channel_id=1, source_target_pairs={{0,1},{1,2},{2,3},{3,4},{4,5},{5,6},{6,7},{7,8},{8,9},{9,10},{10,1... | collective-permute-start | bytes 98312 | tf_op jit(solution)/shard_map/ppermute | solution.py:19
  118.9 4.6 %collective-permute-start.6 = (bf16[8,2048]{1,0:T(8,128)(2,1)S(1)}, bf16[8,2048]{1,0:T(8,128)(2,1)S(1)}, u32[]{:S(2)}, u32[]{:S(2)}) collective-permute-start(bf16[8,2048]{1,0:T(8,128)(2,1)S(1)} %collective-permute-done.4), channel_id=1, source_target_pairs={{0,1},{1,2},{2,3},{3,4},{4,5},{5,6},{6,7},{7,8},{8,9},{9,10},{10,1... | collective-permute-start | bytes 98312 | tf_op jit(solution)/shard_map/ppermute | solution.py:19
  123.4 4.6 %collective-permute-start.8 = (bf16[8,2048]{1,0:T(8,128)(2,1)S(1)}, bf16[8,2048]{1,0:T(8,128)(2,1)S(1)}, u32[]{:S(2)}, u32[]{:S(2)}) collective-permute-start(bf16[8,2048]{1,0:T(8,128)(2,1)S(1)} %collective-permute-done.6), channel_id=1, source_target_pairs={{0,1},{1,2},{2,3},{3,4},{4,5},{5,6},{6,7},{7,8},{8,9},{9,10},{10,1... | collective-permute-start | bytes 98312 | tf_op jit(solution)/shard_map/ppermute | solution.py:19
  123.6 4.6 %collective-permute-start.9 = (bf16[8,2048]{1,0:T(8,128)(2,1)S(1)}, bf16[8,2048]{1,0:T(8,128)(2,1)S(1)}, u32[]{:S(2)}, u32[]{:S(2)}) collective-permute-start(bf16[8,2048]{1,0:T(8,128)(2,1)S(1)} %collective-permute-done.7), channel_id=1, source_target_pairs={{0,15},{1,0},{2,1},{3,2},{4,3},{5,4},{6,5},{7,6},{8,7},{9,8},{10,9... | collective-permute-start | bytes 98312 | tf_op jit(solution)/shard_map/ppermute | solution.py:24
  128.0 4.6 %collective-permute-start.10 = (bf16[8,2048]{1,0:T(8,128)(2,1)S(1)}, bf16[8,2048]{1,0:T(8,128)(2,1)S(1)}, u32[]{:S(2)}, u32[]{:S(2)}) collective-permute-start(bf16[8,2048]{1,0:T(8,128)(2,1)S(1)} %collective-permute-done.8), channel_id=1, source_target_pairs={{0,1},{1,2},{2,3},{3,4},{4,5},{5,6},{6,7},{7,8},{8,9},{9,10},{10,1... | collective-permute-start | bytes 98312 | tf_op jit(solution)/shard_map/ppermute | solution.py:19
  128.2 4.6 %collective-permute-start.11 = (bf16[8,2048]{1,0:T(8,128)(2,1)S(1)}, bf16[8,2048]{1,0:T(8,128)(2,1)S(1)}, u32[]{:S(2)}, u32[]{:S(2)}) collective-permute-start(bf16[8,2048]{1,0:T(8,128)(2,1)S(1)} %collective-permute-done.9), channel_id=1, source_target_pairs={{0,15},{1,0},{2,1},{3,2},{4,3},{5,4},{6,5},{7,6},{8,7},{9,8},{10,9... | collective-permute-start | bytes 98312 | tf_op jit(solution)/shard_map/ppermute | solution.py:24
  132.5 4.6 %collective-permute-start.12 = (bf16[8,2048]{1,0:T(8,128)(2,1)S(1)}, bf16[8,2048]{1,0:T(8,128)(2,1)S(1)}, u32[]{:S(2)}, u32[]{:S(2)}) collective-permute-start(bf16[8,2048]{1,0:T(8,128)(2,1)S(1)} %collective-permute-done.10), channel_id=1, source_target_pairs={{0,1},{1,2},{2,3},{3,4},{4,5},{5,6},{6,7},{7,8},{8,9},{9,10},{10,1... | collective-permute-start | bytes 98312 | tf_op jit(solution)/shard_map/ppermute | solution.py:19
  132.7 5.0 %collective-permute-start.13 = (bf16[8,2048]{1,0:T(8,128)(2,1)S(1)}, bf16[8,2048]{1,0:T(8,128)(2,1)S(1)}, u32[]{:S(2)}, u32[]{:S(2)}) collective-permute-start(bf16[8,2048]{1,0:T(8,128)(2,1)S(1)} %collective-permute-done.11), channel_id=1, source_target_pairs={{0,15},{1,0},{2,1},{3,2},{4,3},{5,4},{6,5},{7,6},{8,7},{9,8},{10,9... | collective-permute-start | bytes 98312 | tf_op jit(solution)/shard_map/ppermute | solution.py:24
  137.1 4.5 %collective-permute-start.14 = (bf16[8,2048]{1,0:T(8,128)(2,1)S(1)}, bf16[8,2048]{1,0:T(8,128)(2,1)S(1)}, u32[]{:S(2)}, u32[]{:S(2)}) collective-permute-start(bf16[8,2048]{1,0:T(8,128)(2,1)S(1)} %collective-permute-done.12), channel_id=1, source_target_pairs={{0,1},{1,2},{2,3},{3,4},{4,5},{5,6},{6,7},{7,8},{8,9},{9,10},{10,1... | collective-permute-start | bytes 98312 | tf_op jit(solution)/shard_map/ppermute | solution.py:19
  142.0 6.6 %collective-permute-start.15 = (bf16[128,128]{0,1:T(8,128)(2,1)S(1)}, bf16[128,128]{0,1:T(8,128)(2,1)S(1)}, u32[]{:S(2)}, u32[]{:S(2)}) collective-permute-start(bf16[128,128]{0,1:T(8,128)(2,1)S(1)} %convolution_convert_fusion.7), channel_id=1, source_target_pairs={{0,1},{1,0},{2,3},{3,2},{4,5},{5,4},{6,7},{7,6},{8,9},{9,8},{10,11... | collective-permute-start | bytes 98312 | tf_op jit(solution)/shard_map/ppermute | solution.py:49
  148.7 5.0 %collective-permute-start.16 = (bf16[128,256]{0,1:T(8,128)(2,1)S(1)}, bf16[128,256]{0,1:T(8,128)(2,1)S(1)}, u32[]{:S(2)}, u32[]{:S(2)}) collective-permute-start(bf16[128,256]{0,1:T(8,128)(2,1)S(1)} %maximum_select_fusion.7), channel_id=1, source_target_pairs={{0,2},{2,0},{1,3},{3,1},{4,6},{6,4},{5,7},{7,5},{8,10},{10,8},{9,1... | collective-permute-start | bytes 196616 | tf_op jit(solution)/shard_map/ppermute | solution.py:49
  182.0 15.9 %collective-permute-start.19 = (bf16[128,4]{0,1:T(4,128)(2,1)S(1)}, bf16[128,4]{0,1:T(4,128)(2,1)S(1)}, u32[]{:S(2)}, u32[]{:S(2)}) collective-permute-start(bf16[128,4]{0,1:T(4,128)(2,1)S(1)} %get-tuple-element.49), channel_id=1, source_target_pairs={{0,1},{1,0},{2,3},{3,2},{4,5},{5,4},{6,7},{7,6},{8,9},{9,8},{10,11... | collective-permute-start | bytes 3080 | tf_op jit(solution)/shard_map/ppermute | solution.py:49
  196.0 4.8 %collective-permute-start.23 = (bf16[128,4]{0,1:T(4,128)(2,1)S(1)}, bf16[128,4]{0,1:T(4,128)(2,1)S(1)}, u32[]{:S(2)}, u32[]{:S(2)}) collective-permute-start(bf16[128,4]{0,1:T(4,128)(2,1)S(1)} %get-tuple-element.50), channel_id=1, source_target_pairs={{0,1},{1,0},{2,3},{3,2},{4,5},{5,4},{6,7},{7,6},{8,9},{9,8},{10,11... | collective-permute-start | bytes 3080 | tf_op jit(solution)/shard_map/ppermute | solution.py:49
  197.9 5.4 %collective-permute-start.21 = (bf16[128,4]{0,1:T(4,128)(2,1)S(1)}, bf16[128,4]{0,1:T(4,128)(2,1)S(1)}, u32[]{:S(2)}, u32[]{:S(2)}) collective-permute-start(bf16[128,4]{0,1:T(4,128)(2,1)S(1)} %fusion.82), channel_id=1, source_target_pairs={{0,2},{2,0},{1,3},{3,1},{4,6},{6,4},{5,7},{7,5},{8,10},{10,8},{9,1... | collective-permute-start | bytes 3080 | tf_op jit(solution)/shard_map/ppermute | solution.py:49
  200.8 4.3 collective-permute-start.24
  207.6 5.3 %collective-permute-start.20 = (bf16[128,4,128]{2,0,1:T(8,128)(2,1)}, bf16[128,4,128]{2,0,1:T(8,128)(2,1)}, u32[]{:S(2)}, u32[]{:S(2)}) collective-permute-start(bf16[128,4,128]{2,0,1:T(8,128)(2,1)} %get-tuple-element.53), channel_id=1, source_target_pairs={{0,1},{1,0},{2,3},{3,2},{4,5},{5,4},{6,7},{7,6},{8,9},{9,8},{10,11... | collective-permute-start | bytes 393224 | tf_op jit(solution)/shard_map/ppermute | solution.py:49
  214.1 6.6 %collective-permute-start.22 = (bf16[128,4,128]{2,0,1:T(8,128)(2,1)S(1)}, bf16[128,4,128]{2,0,1:T(8,128)(2,1)S(1)}, u32[]{:S(2)}, u32[]{:S(2)}) collective-permute-start(bf16[128,4,128]{2,0,1:T(8,128)(2,1)S(1)} %get-tuple-element.27), channel_id=1, source_target_pairs={{0,2},{2,0},{1,3},{3,1},{4,6},{6,4},{5,7},{7,5},{8,10},{10,8},{9,1... | collective-permute-start | bytes 393224 | tf_op jit(solution)/shard_map/ppermute | solution.py:49
  221.9 24.3 %all-to-all-start = ((bf16[16,8,2048]{2,1,0:T(8,128)(2,1)}), bf16[16,8,2048]{2,1,0:T(8,128)(2,1)S(1)}, u32[]{:S(2)}, u32[]{:S(2)}) async-start(bf16[16,8,2048]{2,1,0:T(8,128)(2,1)} %fusion.8), calls=%async_computation | async-start | bytes 1048576 | tf_op jit(solution)/shard_map/all_to_all | solution.py:38
  251.3 4.3 collective-permute-start.29
  255.5 4.6 %collective-permute-start.31 = (bf16[8,2048]{1,0:T(8,128)(2,1)S(1)}, bf16[8,2048]{1,0:T(8,128)(2,1)S(1)}, u32[]{:S(2)}, u32[]{:S(2)}) collective-permute-start(bf16[8,2048]{1,0:T(8,128)(2,1)S(1)} %collective-permute-done.29), channel_id=1, source_target_pairs={{0,1},{1,2},{2,3},{3,4},{4,5},{5,6},{6,7},{7,8},{8,9},{9,10},{10,1... | collective-permute-start | bytes 98312 | tf_op jit(solution)/shard_map/ppermute | solution.py:19
  260.1 4.6 %collective-permute-start.33 = (bf16[8,2048]{1,0:T(8,128)(2,1)S(1)}, bf16[8,2048]{1,0:T(8,128)(2,1)S(1)}, u32[]{:S(2)}, u32[]{:S(2)}) collective-permute-start(bf16[8,2048]{1,0:T(8,128)(2,1)S(1)} %collective-permute-done.31), channel_id=1, source_target_pairs={{0,1},{1,2},{2,3},{3,4},{4,5},{5,6},{6,7},{7,8},{8,9},{9,10},{10,1... | collective-permute-start | bytes 98312 | tf_op jit(solution)/shard_map/ppermute | solution.py:19
  264.6 4.6 %collective-permute-start.35 = (bf16[8,2048]{1,0:T(8,128)(2,1)S(1)}, bf16[8,2048]{1,0:T(8,128)(2,1)S(1)}, u32[]{:S(2)}, u32[]{:S(2)}) collective-permute-start(bf16[8,2048]{1,0:T(8,128)(2,1)S(1)} %collective-permute-done.33), channel_id=1, source_target_pairs={{0,1},{1,2},{2,3},{3,4},{4,5},{5,6},{6,7},{7,8},{8,9},{9,10},{10,1... | collective-permute-start | bytes 98312 | tf_op jit(solution)/shard_map/ppermute | solution.py:19
  264.8 4.6 %collective-permute-start.36 = (bf16[8,2048]{1,0:T(8,128)(2,1)S(1)}, bf16[8,2048]{1,0:T(8,128)(2,1)S(1)}, u32[]{:S(2)}, u32[]{:S(2)}) collective-permute-start(bf16[8,2048]{1,0:T(8,128)(2,1)S(1)} %collective-permute-done.34), channel_id=1, source_target_pairs={{0,15},{1,0},{2,1},{3,2},{4,3},{5,4},{6,5},{7,6},{8,7},{9,8},{10,9... | collective-permute-start | bytes 98312 | tf_op jit(solution)/shard_map/ppermute | solution.py:24
  269.2 4.6 %collective-permute-start.37 = (bf16[8,2048]{1,0:T(8,128)(2,1)S(1)}, bf16[8,2048]{1,0:T(8,128)(2,1)S(1)}, u32[]{:S(2)}, u32[]{:S(2)}) collective-permute-start(bf16[8,2048]{1,0:T(8,128)(2,1)S(1)} %collective-permute-done.35), channel_id=1, source_target_pairs={{0,1},{1,2},{2,3},{3,4},{4,5},{5,6},{6,7},{7,8},{8,9},{9,10},{10,1... | collective-permute-start | bytes 98312 | tf_op jit(solution)/shard_map/ppermute | solution.py:19
  269.4 4.6 %collective-permute-start.38 = (bf16[8,2048]{1,0:T(8,128)(2,1)S(1)}, bf16[8,2048]{1,0:T(8,128)(2,1)S(1)}, u32[]{:S(2)}, u32[]{:S(2)}) collective-permute-start(bf16[8,2048]{1,0:T(8,128)(2,1)S(1)} %collective-permute-done.36), channel_id=1, source_target_pairs={{0,15},{1,0},{2,1},{3,2},{4,3},{5,4},{6,5},{7,6},{8,7},{9,8},{10,9... | collective-permute-start | bytes 98312 | tf_op jit(solution)/shard_map/ppermute | solution.py:24
  273.7 4.6 %collective-permute-start.39 = (bf16[8,2048]{1,0:T(8,128)(2,1)S(1)}, bf16[8,2048]{1,0:T(8,128)(2,1)S(1)}, u32[]{:S(2)}, u32[]{:S(2)}) collective-permute-start(bf16[8,2048]{1,0:T(8,128)(2,1)S(1)} %collective-permute-done.37), channel_id=1, source_target_pairs={{0,1},{1,2},{2,3},{3,4},{4,5},{5,6},{6,7},{7,8},{8,9},{9,10},{10,1... | collective-permute-start | bytes 98312 | tf_op jit(solution)/shard_map/ppermute | solution.py:19
  278.7 6.0 %collective-permute-start.40 = (bf16[2,176]{0,1:T(8,128)(2,1)S(1)}, bf16[2,176]{0,1:T(8,128)(2,1)S(1)}, u32[]{:S(2)}, u32[]{:S(2)}) collective-permute-start(bf16[2,176]{0,1:T(8,128)(2,1)S(1)} %slice.122), channel_id=1, source_target_pairs={{0,16},{16,32},{32,48},{48,64},{64,80},{80,96},{96,112},{112,128},... | collective-permute-start | bytes 2120 | tf_op jit(solution)/shard_map/ppermute | solution.py:64
  287.4 26.4 %all-to-all-start.1 = ((bf16[16,8,2048]{2,1,0:T(8,128)(2,1)}), bf16[16,8,2048]{2,1,0:T(8,128)(2,1)S(1)}, u32[]{:S(2)}, u32[]{:S(2)}) async-start(bf16[16,8,2048]{2,1,0:T(8,128)(2,1)} %fusion.9), calls=%async_computation.1 | async-start | bytes 1048576 | tf_op jit(solution)/shard_map/all_to_all | solution.py:38
  296.5 70.6 %all-gather.8.cloned.1.call-start = ((), (), s32[]{:S(2)}) async-start(), calls=%async_computation.5 | async-start | bytes 2228224 | tf_op jit(solution)/shard_map/all_gather | solution.py:54
  323.0 4.5 %collective-permute-start.48 = (bf16[8,2048]{1,0:T(8,128)(2,1)S(1)}, bf16[8,2048]{1,0:T(8,128)(2,1)S(1)}, u32[]{:S(2)}, u32[]{:S(2)}) collective-permute-start(bf16[8,2048]{1,0:T(8,128)(2,1)S(1)} %collective-permute-done.46), channel_id=1, source_target_pairs={{0,1},{1,2},{2,3},{3,4},{4,5},{5,6},{6,7},{7,8},{8,9},{9,10},{10,1... | collective-permute-start | bytes 98312 | tf_op jit(solution)/shard_map/ppermute | solution.py:19
  327.5 4.6 %collective-permute-start.50 = (bf16[8,2048]{1,0:T(8,128)(2,1)S(1)}, bf16[8,2048]{1,0:T(8,128)(2,1)S(1)}, u32[]{:S(2)}, u32[]{:S(2)}) collective-permute-start(bf16[8,2048]{1,0:T(8,128)(2,1)S(1)} %collective-permute-done.48), channel_id=1, source_target_pairs={{0,1},{1,2},{2,3},{3,4},{4,5},{5,6},{6,7},{7,8},{8,9},{9,10},{10,1... | collective-permute-start | bytes 98312 | tf_op jit(solution)/shard_map/ppermute | solution.py:19
  328.1 4.5 %collective-permute-start.51 = (bf16[8,2048]{1,0:T(8,128)(2,1)S(1)}, bf16[8,2048]{1,0:T(8,128)(2,1)S(1)}, u32[]{:S(2)}, u32[]{:S(2)}) collective-permute-start(bf16[8,2048]{1,0:T(8,128)(2,1)S(1)} %collective-permute-done.49), channel_id=1, source_target_pairs={{0,15},{1,0},{2,1},{3,2},{4,3},{5,4},{6,5},{7,6},{8,7},{9,8},{10,9... | collective-permute-start | bytes 98312 | tf_op jit(solution)/shard_map/ppermute | solution.py:24
  332.1 4.6 %collective-permute-start.52 = (bf16[8,2048]{1,0:T(8,128)(2,1)S(1)}, bf16[8,2048]{1,0:T(8,128)(2,1)S(1)}, u32[]{:S(2)}, u32[]{:S(2)}) collective-permute-start(bf16[8,2048]{1,0:T(8,128)(2,1)S(1)} %collective-permute-done.50), channel_id=1, source_target_pairs={{0,1},{1,2},{2,3},{3,4},{4,5},{5,6},{6,7},{7,8},{8,9},{9,10},{10,1... | collective-permute-start | bytes 98312 | tf_op jit(solution)/shard_map/ppermute | solution.py:19
  332.5 4.6 %collective-permute-start.53 = (bf16[8,2048]{1,0:T(8,128)(2,1)S(1)}, bf16[8,2048]{1,0:T(8,128)(2,1)S(1)}, u32[]{:S(2)}, u32[]{:S(2)}) collective-permute-start(bf16[8,2048]{1,0:T(8,128)(2,1)S(1)} %collective-permute-done.51), channel_id=1, source_target_pairs={{0,15},{1,0},{2,1},{3,2},{4,3},{5,4},{6,5},{7,6},{8,7},{9,8},{10,9... | collective-permute-start | bytes 98312 | tf_op jit(solution)/shard_map/ppermute | solution.py:24
  336.6 4.6 %collective-permute-start.54 = (bf16[8,2048]{1,0:T(8,128)(2,1)S(1)}, bf16[8,2048]{1,0:T(8,128)(2,1)S(1)}, u32[]{:S(2)}, u32[]{:S(2)}) collective-permute-start(bf16[8,2048]{1,0:T(8,128)(2,1)S(1)} %collective-permute-done.52), channel_id=1, source_target_pairs={{0,1},{1,2},{2,3},{3,4},{4,5},{5,6},{6,7},{7,8},{8,9},{9,10},{10,1... | collective-permute-start | bytes 98312 | tf_op jit(solution)/shard_map/ppermute | solution.py:19
  337.1 4.6 %collective-permute-start.55 = (bf16[8,2048]{1,0:T(8,128)(2,1)S(1)}, bf16[8,2048]{1,0:T(8,128)(2,1)S(1)}, u32[]{:S(2)}, u32[]{:S(2)}) collective-permute-start(bf16[8,2048]{1,0:T(8,128)(2,1)S(1)} %collective-permute-done.53), channel_id=1, source_target_pairs={{0,15},{1,0},{2,1},{3,2},{4,3},{5,4},{6,5},{7,6},{8,7},{9,8},{10,9... | collective-permute-start | bytes 98312 | tf_op jit(solution)/shard_map/ppermute | solution.py:24
  341.2 4.6 %collective-permute-start.56 = (bf16[8,2048]{1,0:T(8,128)(2,1)S(1)}, bf16[8,2048]{1,0:T(8,128)(2,1)S(1)}, u32[]{:S(2)}, u32[]{:S(2)}) collective-permute-start(bf16[8,2048]{1,0:T(8,128)(2,1)S(1)} %collective-permute-done.54), channel_id=1, source_target_pairs={{0,1},{1,2},{2,3},{3,4},{4,5},{5,6},{6,7},{7,8},{8,9},{9,10},{10,1... | collective-permute-start | bytes 98312 | tf_op jit(solution)/shard_map/ppermute | solution.py:19
  346.1 6.6 %collective-permute-start.57 = (bf16[128,128]{0,1:T(8,128)(2,1)S(1)}, bf16[128,128]{0,1:T(8,128)(2,1)S(1)}, u32[]{:S(2)}, u32[]{:S(2)}) collective-permute-start(bf16[128,128]{0,1:T(8,128)(2,1)S(1)} %convolution_convert_fusion.6), channel_id=1, source_target_pairs={{0,1},{1,0},{2,3},{3,2},{4,5},{5,4},{6,7},{7,6},{8,9},{9,8},{10,11... | collective-permute-start | bytes 98312 | tf_op jit(solution)/shard_map/ppermute | solution.py:49
  352.7 14.3 %collective-permute-start.58 = (bf16[128,256]{0,1:T(8,128)(2,1)S(1)}, bf16[128,256]{0,1:T(8,128)(2,1)S(1)}, u32[]{:S(2)}, u32[]{:S(2)}) collective-permute-start(bf16[128,256]{0,1:T(8,128)(2,1)S(1)} %maximum_select_fusion.9), channel_id=1, source_target_pairs={{0,2},{2,0},{1,3},{3,1},{4,6},{6,4},{5,7},{7,5},{8,10},{10,8},{9,1... | collective-permute-start | bytes 196616 | tf_op jit(solution)/shard_map/ppermute | solution.py:49
  371.4 16.8 %collective-permute-start.59 = (bf16[128,4]{0,1:T(4,128)(2,1)S(1)}, bf16[128,4]{0,1:T(4,128)(2,1)S(1)}, u32[]{:S(2)}, u32[]{:S(2)}) collective-permute-start(bf16[128,4]{0,1:T(4,128)(2,1)S(1)} %get-tuple-element.46), channel_id=1, source_target_pairs={{0,1},{1,0},{2,3},{3,2},{4,5},{5,4},{6,7},{7,6},{8,9},{9,8},{10,11... | collective-permute-start | bytes 3080 | tf_op jit(solution)/shard_map/ppermute | solution.py:49
  386.2 4.5 %collective-permute-start.63 = (bf16[128,4]{0,1:T(4,128)(2,1)S(1)}, bf16[128,4]{0,1:T(4,128)(2,1)S(1)}, u32[]{:S(2)}, u32[]{:S(2)}) collective-permute-start(bf16[128,4]{0,1:T(4,128)(2,1)S(1)} %get-tuple-element.47), channel_id=1, source_target_pairs={{0,1},{1,0},{2,3},{3,2},{4,5},{5,4},{6,7},{7,6},{8,9},{9,8},{10,11... | collective-permute-start | bytes 3080 | tf_op jit(solution)/shard_map/ppermute | solution.py:49
  388.2 5.4 %collective-permute-start.61 = (bf16[128,4]{0,1:T(4,128)(2,1)S(1)}, bf16[128,4]{0,1:T(4,128)(2,1)S(1)}, u32[]{:S(2)}, u32[]{:S(2)}) collective-permute-start(bf16[128,4]{0,1:T(4,128)(2,1)S(1)} %fusion.83), channel_id=1, source_target_pairs={{0,2},{2,0},{1,3},{3,1},{4,6},{6,4},{5,7},{7,5},{8,10},{10,8},{9,1... | collective-permute-start | bytes 3080 | tf_op jit(solution)/shard_map/ppermute | solution.py:49
  390.7 4.3 collective-permute-start.64
  396.8 4.8 %collective-permute-start.60 = (bf16[128,4,128]{2,0,1:T(8,128)(2,1)S(1)}, bf16[128,4,128]{2,0,1:T(8,128)(2,1)S(1)}, u32[]{:S(2)}, u32[]{:S(2)}) collective-permute-start(bf16[128,4,128]{2,0,1:T(8,128)(2,1)S(1)} %get-tuple-element.57), channel_id=1, source_target_pairs={{0,1},{1,0},{2,3},{3,2},{4,5},{5,4},{6,7},{7,6},{8,9},{9,8},{10,11... | collective-permute-start | bytes 393224 | tf_op jit(solution)/shard_map/ppermute | solution.py:49
  401.8 6.6 %collective-permute-start.62 = (bf16[128,4,128]{2,0,1:T(8,128)(2,1)S(1)}, bf16[128,4,128]{2,0,1:T(8,128)(2,1)S(1)}, u32[]{:S(2)}, u32[]{:S(2)}) collective-permute-start(bf16[128,4,128]{2,0,1:T(8,128)(2,1)S(1)} %get-tuple-element.12), channel_id=1, source_target_pairs={{0,2},{2,0},{1,3},{3,1},{4,6},{6,4},{5,7},{7,5},{8,10},{10,8},{9,1... | collective-permute-start | bytes 393224 | tf_op jit(solution)/shard_map/ppermute | solution.py:49
  (40 other events, 1650.1 us)
Sparse Core Ops, SparseCore 0:
  9.8 83.0 all-gather.3
  107.9 69.7 all-gather.5
  299.4 67.6 all-gather.7
